TPU v7x, 256 devices: a whole 4x4x8 slice. The times are simulated.
256 devices in a mesh: sp: 64 (over z, x, core), tp: 4 (over y).
Axes of the slice: x: 4, y: 4, z: 8, core: 2. Of those that a mesh axis runs over, the one named last changes fastest.
Arguments:
- stream: bfloat16 [32768, 2048], P(('sp', 'tp')), may hold values from -6 to 6
- queries: bfloat16 [32768, 512], P('sp', 'tp'), may hold values from -6 to 6
- key_rows: bfloat16 [32768, 512], P('sp', 'tp'), may hold values from -6 to 6
- values: bfloat16 [32768, 1024], P('sp', 'tp'), may hold values from -6 to 6
- out_gate: bfloat16 [32768, 1024], P('sp', 'tp'), may hold values from -6 to 6
- fwd_decay: float32 [32768, 512], P('sp', 'tp'), may hold values from -14 to 14
- bwd_decay: float32 [32768, 512], P('sp', 'tp'), may hold values from -14 to 14
- head_gain: float32 [1024], P('tp'), may hold values from 0.1 to 1.9
- out_proj: bfloat16 [1024, 2048], replicated, may hold values from -0.1875 to 0.1875
- mix_gain: float32 [2048], replicated, may hold values from 0.1 to 1.9
- ffn_gain: float32 [2048], replicated, may hold values from 0.1 to 1.9
- moe_gain: float32 [2048], replicated, may hold values from 0.1 to 1.9
- routes: int32 [32768, 2], P(('sp', 'tp')), may hold values from 0 to 63, all different within a row; in each aligned block of 128 rows (0 to 127, 128 to 255, ...) at most 6 rows name the same one
- route_weight: float32 [32768, 2], P(('sp', 'tp')), may hold values from 0.25 to 2.5
- expert_gate: bfloat16 [64, 2048, 1024], P('sp', None, 'tp'), may hold values from -0.125 to 0.125
- expert_up: bfloat16 [64, 2048, 1024], P('sp', None, 'tp'), may hold values from -0.125 to 0.125
- expert_down: bfloat16 [64, 1024, 2048], P('sp', 'tp'), may hold values from -0.1875 to 0.1875
- shared_gate: bfloat16 [2048, 512], P(None, 'tp'), may hold values from -0.125 to 0.125
- shared_up: bfloat16 [2048, 512], P(None, 'tp'), may hold values from -0.125 to 0.125
- shared_down: bfloat16 [512, 2048], P('tp'), may hold values from -0.25 to 0.25
Outputs:
- updated: bfloat16 [32768, 2048], P(('sp', 'tp'))
Inputs may be any that keep to these rules, and one draw needn't show every extreme that they name: `routes`: each row names 2 different experts. Among the rows of one device no expert is named more than 6 times, and in every draw some device names some expert exactly 6 times.
All inputs are finite; a program needn't handle non-finite values.
Results may differ from a plain program's by a relative error of at most 0.023.
Values may be sent and summed in bfloat16 or wider, within the bound.
No kernel may reach another device: no remote copies, remote signals or barrier semaphores. Data moves between devices by JAX's collectives and lax.ppermute only.
A program may use at most 128 MiB of HBM per device.

v0:
```python
import jax
import jax.numpy as jnp
from jax import lax
from jax.sharding import Mesh
from jax.sharding import PartitionSpec as P

KEY_CHANNELS = 64
DV = 128
BLK = 64
TOPK = 2
SP = ("sp_0", "sp_1", "sp_2")
SP_TP = ("sp_0", "sp_1", "sp_2", "tp")
EPS = 1e-06
GATE_NORM = 16.0
ROPE_BASE = 10000.0


def gathered_once(array, axis):
    leaves = jax.tree.leaves(array)
    sequence = sorted(range(len(leaves)), key=lambda k: -leaves[k].size)
    width = (1, *leaves[sequence[0]].shape)[-1]
    lines = [
        jnp.pad(leaves[k].reshape(-1), (0, -leaves[k].size % width)).reshape(-1, width)
        for k in sequence
    ]
    both, at, found = (lax.all_gather(jnp.concatenate(lines), axis), 0, {})
    for k, line in zip(sequence, lines):
        share = both[:, at : at + len(line)].reshape(len(both), -1)
        found[k] = share[:, : leaves[k].size].reshape(-1, *leaves[k].shape)
        at += len(line)
    numbers = iter(range(len(leaves)))
    return jax.tree.map(lambda _: found[next(numbers)], array)


def prefix(array, axis, combine, identity):
    length, position = (lax.axis_size(axis), lax.axis_index(axis))
    everything = gathered_once(
        jax.tree.map(
            lambda part, kind: part.astype(kind),
            array,
            jax.tree.map(lambda a: jnp.bfloat16 if a.dtype == jnp.float32 else a.dtype, array),
        ),
        axis,
    )
    start = jax.tree.map(
        lambda part, zero: jnp.broadcast_to(jnp.asarray(zero, part.dtype), part.shape),
        array,
        identity,
    )

    def step(k, before):
        reached = k < position
        new = combine(
            before, jax.tree.map(lambda part, own: part[k].astype(own.dtype), everything, array)
        )
        return jax.tree.map(lambda a, b: jnp.where(reached, a, b), new, before)

    return lax.fori_loop(0, length, step, start)


def neutral_like(array, identity):
    return jax.tree.map(
        lambda a, e: jnp.broadcast_to(jnp.asarray(e, a.dtype), a.shape), array, identity
    )


def entering(array, axes, combine, identity):
    before = start = neutral_like(array, identity)
    so_far = array
    for axis in reversed(axes):
        length, position = (lax.axis_size(axis), lax.axis_index(axis))
        pieces = gathered_once(
            jax.tree.map(
                lambda part, kind: part.astype(kind),
                so_far,
                jax.tree.map(lambda a: jnp.bfloat16 if a.dtype == jnp.float32 else a.dtype, array),
            ),
            axis,
        )
        inside, so_far = (start, start)
        for k in reversed(range(length)):
            passed = k > position
            so_far = combine(
                so_far, jax.tree.map(lambda part, own: part[k].astype(own.dtype), pieces, array)
            )
            inside = jax.tree.map(lambda new, old: jnp.where(passed, new, old), so_far, inside)
        before = combine(inside, before)
    return before


def normalize(tensor):
    return tensor * lax.rsqrt(jnp.mean(tensor * tensor, axis=-1, keepdims=True) + EPS)


def rotate(tensor, positions):
    half_width = tensor.shape[-1] // 2
    frequency = ROPE_BASE ** (-jnp.arange(half_width, dtype=jnp.float32) / half_width)
    angles = positions[:, None] * frequency[None, :]
    cosine = jnp.cos(angles)[:, None, :]
    sine_part = jnp.sin(angles)[:, None, :]
    front_half = tensor[..., :half_width]
    back_half = tensor[..., half_width:]
    return jnp.concatenate(
        [front_half * cosine - back_half * sine_part, front_half * sine_part + back_half * cosine],
        axis=-1,
    )


def blockwise(query_rows, key_data, value_matrix, log_decay, start_state):
    length, head_count, key_width = query_rows.shape
    value_width = value_matrix.shape[-1]
    block_count = length // BLK
    query_blocks = query_rows.reshape(block_count, BLK, head_count, key_width)
    key_blocks = key_data.reshape(block_count, BLK, head_count, key_width)
    value_blocks = value_matrix.reshape(block_count, BLK, head_count, value_width)
    cumul = jnp.cumsum(log_decay.reshape(block_count, BLK, head_count, key_width), axis=1)
    middle = cumul[:, BLK // 2 - 1 : BLK // 2]
    query_scaled = query_blocks * jnp.exp(cumul - middle)
    key_scaled = key_blocks * jnp.exp(middle - cumul)
    scores = jnp.einsum("nthk,nshk->nhts", query_scaled, key_scaled)
    lower_mask = jnp.arange(BLK)[:, None] >= jnp.arange(BLK)[None, :]
    scores = jnp.where(lower_mask, scores, 0.0)
    within = jnp.einsum("nhts,nshv->nthv", scores, value_blocks)
    last_cumul = cumul[:, -1:]
    query_in = query_blocks * jnp.exp(cumul)
    key_out = key_blocks * jnp.exp(last_cumul - cumul)
    block_decay = jnp.exp(last_cumul[:, 0])

    def advance(carried_state, pieces):
        query_segment, key_segment, value_segment, decay_segment = pieces
        across_blocks = jnp.einsum("asu,sun->asn", query_segment, carried_state)
        carried_state = carried_state * decay_segment[:, :, None] + jnp.einsum(
            "jco,jcm->com", key_segment, value_segment
        )
        return (carried_state, across_blocks)

    final_state, across_blocks = lax.scan(
        advance, start_state, (query_in, key_out, value_blocks, block_decay)
    )
    return ((within + across_blocks).reshape(length, head_count, value_width), final_state)


def readout(query_rows, log_decay, carried_state):
    cumul = jnp.cumsum(log_decay, axis=0)
    return jnp.einsum("asu,sun->asn", query_rows * jnp.exp(cumul), carried_state)


def compose(earlier, later):
    return (earlier[0] * later[0], earlier[1] * later[0][:, :, None] + later[1])


def feed_forward(row_data, gate_mat, up_mat, down_mat):
    hidden = (
        jax.nn.silu(jnp.dot(row_data, gate_mat, preferred_element_type=jnp.float32))
        * jnp.dot(row_data, up_mat, preferred_element_type=jnp.float32)
    ).astype(jnp.bfloat16)
    return jnp.dot(hidden, down_mat, preferred_element_type=jnp.float32)


def place_slots(route_block, experts):
    flat_ids = route_block.reshape(-1)
    onehot = (flat_ids[:, None] == jnp.arange(experts, dtype=jnp.int32)[None, :]).astype(jnp.int32)
    before = jnp.cumsum(onehot, axis=0) - onehot
    return (flat_ids, jnp.sum(before * onehot, axis=1))


def fill_slots(row_data, route_block, experts, capacity):
    flat_ids, slot_ids = place_slots(route_block, experts)
    token_ids = jnp.arange(flat_ids.shape[0], dtype=jnp.int32) // route_block.shape[1]
    buffer = jnp.zeros((experts, capacity, row_data.shape[1]), row_data.dtype)
    return buffer.at[flat_ids, slot_ids].set(row_data[token_ids])


def body(
    stream,
    queries,
    key_rows,
    values,
    out_gate,
    fwd_decay,
    bwd_decay,
    head_gain,
    out_proj,
    mix_gain,
    ffn_gain,
    moe_gain,
    routes,
    route_weight,
    expert_gate,
    expert_up,
    expert_down,
    shared_gate,
    shared_up,
    shared_down,
):
    tokens_here = stream.shape[0]
    span_rows = queries.shape[0]
    heads_here = queries.shape[1] // KEY_CHANNELS
    offset = lax.axis_index(SP) * span_rows
    positions = (offset + jnp.arange(span_rows, dtype=jnp.int32)).astype(jnp.float32)
    query_rows = rotate(
        queries.astype(jnp.float32).reshape(span_rows, heads_here, KEY_CHANNELS)
        * KEY_CHANNELS ** (-0.5),
        positions,
    )
    key_data = rotate(
        key_rows.astype(jnp.float32).reshape(span_rows, heads_here, KEY_CHANNELS), positions
    )
    value_matrix = values.astype(jnp.float32).reshape(span_rows, heads_here, DV)
    fwd_log = jax.nn.log_sigmoid(fwd_decay).reshape(span_rows, heads_here, KEY_CHANNELS) / GATE_NORM
    bwd_log = (
        jax.nn.log_sigmoid(bwd_decay[::-1]).reshape(span_rows, heads_here, KEY_CHANNELS) / GATE_NORM
    )
    query_back = query_rows[::-1]
    key_back = key_data[::-1]
    value_back = value_matrix[::-1]
    zero_state = jnp.zeros((heads_here, KEY_CHANNELS, DV), jnp.float32)
    identity = (jnp.ones((heads_here, KEY_CHANNELS), jnp.float32), zero_state)
    fwd_out, fwd_final = blockwise(query_rows, key_data, value_matrix, fwd_log, zero_state)
    bwd_out, bwd_final = blockwise(query_back, key_back, value_back, bwd_log, zero_state)
    fwd_summary = (jnp.exp(jnp.sum(fwd_log, axis=0)), fwd_final)
    bwd_summary = (jnp.exp(jnp.sum(bwd_log, axis=0)), bwd_final)
    fwd_carry = prefix(fwd_summary, SP, compose, identity)[1]
    bwd_carry = entering(bwd_summary, SP, compose, identity)[1]
    fwd_out = fwd_out + readout(query_rows, fwd_log, fwd_carry)
    bwd_out = bwd_out + readout(query_back, bwd_log, bwd_carry)
    combined = normalize(fwd_out + bwd_out[::-1]) * head_gain.reshape(heads_here, DV)
    head_mixed = (
        combined.reshape(span_rows, -1) * jax.nn.silu(out_gate.astype(jnp.float32))
    ).astype(jnp.bfloat16)
    mixed_out = lax.all_to_all(head_mixed, "tp", split_axis=0, concat_axis=1, tiled=True)
    projected = jnp.dot(mixed_out, out_proj, preferred_element_type=jnp.float32)
    residual = (stream.astype(jnp.float32) + normalize(projected) * mix_gain).astype(jnp.bfloat16)
    normed = (normalize(residual.astype(jnp.float32)) * ffn_gain).astype(jnp.bfloat16)
    experts = lax.axis_size(SP)
    groups = lax.axis_size("tp")
    capacity = max(2, 3 * tokens_here * TOPK // (2 * experts))
    model_width = normed.shape[1]
    arrived = lax.all_to_all(
        fill_slots(normed, routes, experts, capacity), SP, split_axis=0, concat_axis=0, tiled=True
    )
    fanned, shared_flat = (
        lax.all_gather(arrived.reshape(experts * capacity, model_width), "tp", axis=0, tiled=True),
        lax.all_gather(normed, "tp", axis=0, tiled=True),
    )
    routed_rows = fanned.reshape(groups, experts * capacity, model_width)
    shared_rows = shared_flat.reshape(groups, tokens_here, model_width)
    width_rows = experts * capacity + tokens_here
    number = width_rows * lax.axis_size("tp") // width_rows
    routed_part = routed_rows.reshape(number * experts * capacity, model_width)
    shared_part = shared_rows.reshape(number * tokens_here, model_width)
    routed_out = feed_forward(routed_part, expert_gate[0], expert_up[0], expert_down[0]).reshape(
        number, experts * capacity, model_width
    )
    shared_out = feed_forward(shared_part, shared_gate, shared_up, shared_down).reshape(
        number, tokens_here, model_width
    )
    summed = lax.psum_scatter(
        jnp.concatenate([routed_out, shared_out], axis=1)
        .reshape(width_rows * lax.axis_size("tp"), model_width)
        .astype(jnp.bfloat16),
        "tp",
        scatter_dimension=0,
        tiled=True,
    ).astype(jnp.float32)
    routed_done = (
        summed[: experts * capacity].astype(jnp.bfloat16).reshape(experts, capacity, model_width)
    )
    routed_back = lax.all_to_all(routed_done, SP, split_axis=0, concat_axis=0, tiled=True)
    shared_sum = summed[experts * capacity :]
    flat_ids, slot_ids = place_slots(routes, experts)
    picked = routed_back.reshape(experts * capacity, model_width)[flat_ids * capacity + slot_ids]
    picked = picked.astype(jnp.float32).reshape(tokens_here, TOPK, model_width)
    mixture = shared_sum + jnp.sum(picked * route_weight[:, :, None], axis=1)
    return (residual.astype(jnp.float32) + normalize(mixture) * moe_gain).astype(jnp.bfloat16)


def solution(mesh):
    finer = Mesh(mesh.devices.reshape(8, 4, 2, mesh.shape["tp"]), ("sp_0", "sp_1", "sp_2", "tp"))
    placed = (
        P(SP_TP, None),
        P(SP, "tp"),
        P(SP, "tp"),
        P(SP, "tp"),
        P(SP, "tp"),
        P(SP, "tp"),
        P(SP, "tp"),
        P("tp"),
        P(),
        P(),
        P(),
        P(),
        P(SP_TP, None),
        P(SP_TP, None),
        P(SP, None, "tp"),
        P(SP, None, "tp"),
        P(SP, "tp", None),
        P(None, "tp"),
        P(None, "tp"),
        P("tp", None),
    )
    return jax.shard_map(
        body, mesh=finer, in_specs=placed, out_specs=P(SP_TP, None), check_vma=False
    )
```

profile of v0, /device:TPU:2, one launch (start us, length us, event | category | flops | bytes accessed | tf_op | source)
XLA Modules:
  0.0 553.1 jit_solution(17728160664577737282)
XLA Ops:
  10.0 13.0 %fusion.178 = f32[8,64,2,64]{3,0,1,2:T(8,128)S(1)} fusion(f32[8,64,2,64]{3,0,1,2:T(8,128)S(1)} %copy.134), kind=kOutput, calls=%fused_computation.308 | output fusion | flops 4128768 | bytes 524288 | tf_op jit(solution)/shard_map/jit(cumsum)/reduce_window_sum | solution.py:116
  36.9 24.3 %while.40 = (s32[]{:T(128)}, f32[2,64,128]{2,1,0:T(8,128)S(1)}, f32[8,64,2,128]{3,1,2,0:T(8,128)}, f32[8,2,64]{2,0,1:T(8,128)S(1)}, f32[8,64,2,64]{3,0,1,2:T(8,1...) while((s32[]{:T(128)}, f32[2,64,128]{2,1,0:T(8,128)S(1)}, ...), condition=%wide.region_2.3_spmd.clone, body=%wide.region_1.2_spmd.clone.sunk | while | flops 4259843 | bytes 494192 | solution.py:137
  63.6 3.1 rev.15
  66.7 3.1 rev.17
  83.2 24.4 %while.42 = (s32[]{:T(128)}, f32[2,64,128]{2,1,0:T(8,128)S(1)}, f32[8,64,2,128]{3,1,2,0:T(8,128)}, f32[8,2,64]{2,0,1:T(8,128)S(1)}, f32[8,64,2,64]{3,0,1,2:T(8,1...) while((s32[]{:T(128)}, f32[2,64,128]{2,1,0:T(8,128)S(1)}, ...), condition=%wide.region_10.11_spmd.clone, body=%wide.region_9.10_spmd.clone.sunk | while | flops 4259843 | bytes 494192 | solution.py:137
  116.6 12.1 %all-gather.6 = bf16[4,129,128]{2,1,0:T(8,128)(2,1)S(1)} all-gather(bf16[1,129,128]{2,1,0:T(8,128)(2,1)S(1)} %maximum_bitcast_fusion.2), channel_id=4, replica_groups=mesh['sp_0'=8,'sp_1'=4,'sp_2'=2,'tp'=4] {'sp_1'}, dimensions={0}, use_global_device_ids=true | all-gather | bytes 165120 | tf_op jit(solution)/shard_map/all_gather | solution.py:26
  129.3 28.6 %all-gather.7 = bf16[8,129,128]{2,1,0:T(8,128)(2,1)S(1)} all-gather(bf16[1,129,128]{2,1,0:T(8,128)(2,1)S(1)} %maximum_bitcast_fusion.3), channel_id=5, replica_groups=mesh['sp_0'=8,'sp_1'=4,'sp_2'=2,'tp'=4] {'sp_0'}, dimensions={0}, use_global_device_ids=true | all-gather | bytes 297216 | tf_op jit(solution)/shard_map/all_gather | solution.py:26
  167.0 3.0 rev.19
  176.4 8.8 %while.41 = (s32[]{:T(128)}, f32[2,64,128]{2,1,0:T(8,128)S(1)}, s32[]{:T(128)}, bf16[64,2,64]{2,1,0:T(2,128)(2,1)S(1)}, bf16[64,2,64,128]{3,2,1,0:T(8,128)(2,1)S(1)}, /*index=5*/s32[]{:T(128)}, s32[]{:T(128)}) while((s32[]{:T(128)}, f32[2,64,128]{2,1,0:T(8,128)S(1)}, s32[]{:T(128)}, bf16[64,2,64]{2,1,0:T(2,128)(2,1)S(1)}, ...), condition=%wide.region_5.6_spmd.clone, body=%wide.region_4.5_spmd.clone.sunk | while | flops 82052 | bytes 165225 | solution.py:58
  188.2 4.4 all-to-all-start
  192.6 6.7 %all-to-all-done = bf16[4,128,256]{2,1,0:T(8,128)(2,1)S(1)} async-done(((bf16[4,128,256]{2,1,0:T(8,128)(2,1)}), bf16[4,128,256]{2,1,0:T(8,128)(2,1)S(1)}, u32[]{:S(2)}, u32[]{:S(2)}) %all-to-all-start) | async-done | bytes 262176 | tf_op jit(solution)/shard_map/all_to_all | solution.py:231
  199.5 3.1 multiply_reduce_fusion.2
  208.3 33.6 %scatter_fusion = bf16[64,6,2048]{2,0,1:T(8,128)(2,1)S(1)} fusion(bf16[64,6,2048]{2,0,1:T(8,128)(2,1)S(1)} %broadcast_in_dim.40, s32[256]{0:T(256)S(1)} %bitcast.315, bf16[256,2048]{1,0:T(8,128)(2,1)} %gather_fusion), kind=kCustom, calls=%fused_computation.2 | custom fusion | bytes 3147776 | tf_op jit(solution)/shard_map/scatter | solution.py:171
  242.8 59.3 %all_to_all.29 = bf16[64,6,2048]{2,1,0:T(8,128)(2,1)S(1)} all-to-all(bf16[64,6,2048]{2,1,0:T(8,128)(2,1)S(1)} %copy.181), channel_id=1, replica_groups=mesh['sp_0'=8,'sp_1'=4,'sp_2'=2,'tp'=4] {'sp_0','sp_1','sp_2'}, dimensions={0} | all-to-all | bytes 3145728 | tf_op jit(solution)/shard_map/all_to_all | solution.py:239
  306.3 4.9 convolution_convert_fusion.1
  311.1 55.2 %all-gather.12.cloned.1.call-done = bf16[1536,2048]{1,0:T(8,128)(2,1)} async-done(((bf16[384,2048]{1,0:T(8,128)(2,1)}), bf16[1536,2048]{1,0:T(8,128)(2,1)}) %all-gather.12.cloned.1.call-update) | async-done | bytes 6291472 | tf_op jit(solution)/shard_map/all_gather | solution.py:243
  366.4 5.0 fusion.32
  373.5 4.5 convolution_convert_fusion
  378.1 7.6 %pad_maximum_fusion = bf16[4,512,2048]{2,1,0:T(8,128)(2,1)} fusion(bf16[4,128,2048]{2,1,0:T(8,128)(2,1)S(1)} %bitcast.316, bf16[4,384,2048]{2,1,0:T(8,128)(2,1)} %convolution_convert_fusion), kind=kLoop, calls=%fused_computation.32 | loop fusion | flops 16777216 | bytes 16777216 | tf_op jit(solution)/shard_map/concatenate | solution.py:259
  385.7 83.9 %reduce-scatter.2.cloned.1.call-done = bf16[512,2048]{1,0:T(8,128)(2,1)} async-done(((bf16[2048,2048]{1,0:T(8,128)(2,1)}), bf16[512,2048]{1,0:T(8,128)(2,1)}) %reduce-scatter.2.cloned.1.call-update) | async-done | bytes 2097168 | tf_op jit(solution)/shard_map/reduce_scatter | solution.py:258
  472.6 10.9 %all-to-all-start.2 = ((bf16[64,6,2048]{2,1,0:T(8,128)(2,1)}), bf16[64,6,2048]{2,1,0:T(8,128)(2,1)}, u32[]{:S(2)}, u32[]{:S(2)}) async-start(bf16[64,6,2048]{2,1,0:T(8,128)(2,1)} %reshape.770), calls=%async_computation.3 | async-start | bytes 4194304 | tf_op jit(solution)/shard_map/all_to_all | solution.py:269
  483.6 51.0 %all-to-all-done.2 = bf16[64,6,2048]{2,1,0:T(8,128)(2,1)} async-done(((bf16[64,6,2048]{2,1,0:T(8,128)(2,1)}), bf16[64,6,2048]{2,1,0:T(8,128)(2,1)}, u32[]{:S(2)}, u32[]{:S(2)}) %all-to-all-start.2) | async-done | bytes 1572896 | tf_op jit(solution)/shard_map/all_to_all | solution.py:269
  534.6 2.6 reshape.771
  542.0 3.2 multiply_reduce_fusion
  (409 shorter events, 137.4 us)
Async XLA Ops:
  6.5 367.0 %copy-start = (bf16[1,256,2048]{2,1,0:T(8,128)(2,1)S(1)}, bf16[1,256,2048]{2,1,0:T(8,128)(2,1)}, u32[]{:S(2)}) copy-start(bf16[1,256,2048]{2,1,0:T(8,128)(2,1)} %param.42) | copy-start | bytes 3145732
  6.5 167.2 %all-gather.16.cloned.1.call-start = ((), (), s32[]{:S(2)}) async-start(), calls=%async_computation.7 | async-start | bytes 2263040 | tf_op jit(solution)/shard_map/all_gather | solution.py:26
  9.2 13.9 %copy-start.21 = (bf16[512,128]{1,0:T(8,128)(2,1)S(1)}, bf16[512,128]{1,0:T(8,128)(2,1)}, u32[]{:S(2)}) copy-start(bf16[512,128]{1,0:T(8,128)(2,1)} %param.27) | copy-start | bytes 393220
  9.2 14.1 %copy-start.22 = (bf16[512,128]{1,0:T(8,128)(2,1)S(1)}, bf16[512,128]{1,0:T(8,128)(2,1)}, u32[]{:S(2)}) copy-start(bf16[512,128]{1,0:T(8,128)(2,1)} %param.28) | copy-start | bytes 393220
  9.6 13.5 %copy-start.7 = (f32[512,128]{0,1:T(8,128)}, f32[512,128]{0,1:T(8,128)S(1)}, u32[]{:S(2)}) copy-start(f32[512,128]{0,1:T(8,128)S(1)} %get-tuple-element.357) | copy-start | bytes 786436
  9.6 60.2 %copy-start.9 = (f32[512,128]{0,1:T(8,128)}, f32[512,128]{0,1:T(8,128)S(1)}, u32[]{:S(2)}) copy-start(f32[512,128]{0,1:T(8,128)S(1)} %get-tuple-element.416) | copy-start | bytes 786436
  23.9 5.2 copy-start.15
  23.9 5.2 copy-start.16
  74.9 4.5 copy-start.12
  82.4 25.3 %copy-start.18 = (bf16[8,64,2,128]{3,2,1,0:T(2,128)(2,1)S(1)}, bf16[8,64,2,128]{3,2,1,0:T(2,128)(2,1)}, u32[]{:S(2)}) copy-start(bf16[8,64,2,128]{3,2,1,0:T(2,128)(2,1)} %reshape_reshape.8) | copy-start | bytes 786436
  83.2 26.8 %copy-start.26 = (s32[128,2]{0,1:T(2,128)S(1)}, s32[128,2]{0,1:T(2,128)}, u32[]{:S(2)}) copy-start(s32[128,2]{0,1:T(2,128)} %param.38) | copy-start | bytes 3076
  162.0 4.0 copy-start.11
  165.0 5.0 copy-start.8
  174.8 12.2 %copy-start.27 = (f32[256]{0:T(256)S(1)}, f32[256]{0:T(256)}, u32[]{:S(2)}) copy-start(f32[256]{0:T(256)} %param.33) | copy-start | bytes 3076
  188.2 11.1 %all-to-all-start = ((bf16[4,128,256]{2,1,0:T(8,128)(2,1)}), bf16[4,128,256]{2,1,0:T(8,128)(2,1)S(1)}, u32[]{:S(2)}, u32[]{:S(2)}) async-start(bf16[4,128,256]{2,1,0:T(8,128)(2,1)} %bitcast.62), calls=%async_computation | async-start | bytes 524288 | tf_op jit(solution)/shard_map/all_to_all | solution.py:231
  192.6 111.1 %all-gather.14.cloned.1.call-start = ((), (), s32[]{:S(2)}) async-start(), calls=%async_computation.5 | async-start | bytes 2621440 | tf_op jit(solution)/shard_map/all_gather | solution.py:244
  204.8 161.6 %all-gather.12.cloned.1.call-start = ((), (), s32[]{:S(2)}) async-start(), calls=%async_computation.4 | async-start | bytes 7864320 | tf_op jit(solution)/shard_map/all_gather | solution.py:243
  303.7 166.0 %reduce-scatter.2.cloned.1.call-start = ((), (), s32[]{:S(2)}) async-start(), calls=%async_computation.6 | async-start | bytes 10485760 | tf_op jit(solution)/shard_map/reduce_scatter | solution.py:258
  311.1 60.3 %copy-start.30 = (bf16[1,2048,256]{2,1,0:T(8,128)(2,1)S(1)}, bf16[1,2048,256]{2,1,0:T(8,128)(2,1)}, u32[]{:S(2)}) copy-start(bf16[1,2048,256]{2,1,0:T(8,128)(2,1)} %param.41) | copy-start | bytes 3145732
  366.4 5.1 copy-start.29
  373.5 4.5 copy-start.3
  472.6 10.9 %copy-start.28 = (f32[128,2]{0,1:T(2,128)S(1)}, f32[128,2]{0,1:T(2,128)}, u32[]{:S(2)}) copy-start(f32[128,2]{0,1:T(2,128)} %param.39) | copy-start | bytes 3076
  472.6 62.0 %all-to-all-start.2 = ((bf16[64,6,2048]{2,1,0:T(8,128)(2,1)}), bf16[64,6,2048]{2,1,0:T(8,128)(2,1)}, u32[]{:S(2)}, u32[]{:S(2)}) async-start(bf16[64,6,2048]{2,1,0:T(8,128)(2,1)} %reshape.770), calls=%async_computation.3 | async-start | bytes 4194304 | tf_op jit(solution)/shard_map/all_to_all | solution.py:269
  542.0 3.5 copy-start.6
  (15 other events, 29.9 us)
Sparse Core Ops, SparseCore 0:
  62.0 79.3 all-gather.15
  204.9 30.5 all-gather.13
  303.8 62.5 all-gather.11
  385.8 83.7 reduce-scatter.1
where the time goes:
time: 557 us; the launch traced here: 553 us
  waiting for transfers between devices  197 us (35%)
  local copies, waits for them, and re-layouts  119 us (21%)
  blocking collectives  102 us (18%)
  matrix products  56.2 us (10%)
  other arithmetic  46.9 us (8%)
  starting transfers between devices  15.3 us (3%)
  between operations  14 us (3%)
    reduce_scatter x1, waiting for transfers between devices, body(): lax.psum_scatter(jnp.concatenate([routed_out, shared_out], axis=1).reshap...  83.9 us
    all_to_all x1, blocking collectives, body(): lax.all_to_all(fill_slots(normed, routes, experts, capacity), SP, split_a...  59.3 us
    all_gather x1, waiting for transfers between devices, body(): lax.all_gather(arrived.reshape(experts * capacity, model_width), 'tp', ax...  55.2 us
    all_to_all x1, waiting for transfers between devices, body(): lax.all_to_all(routed_done, SP, split_axis=0, concat_axis=0, tiled=True)  51 us
    all_gather x3, blocking collectives, gathered_once(): both, at, found = (lax.all_gather(jnp.concatenate(lines), axis), 0, {})  42.6 us
    scatter x2, local copies, waits for them, and re-layouts, fill_slots(): return buffer.at[flat_ids, slot_ids].set(row_data[token_ids])  34.5 us
    dynamic_slice x32, local copies, waits for them, and re-layouts, blockwise(): lax.scan(advance, start_state, (query_in, key_out, value_blocks, block_de...  20.9 us
    dot_general x16, matrix products, advance(): jnp.einsum('jco,jcm->com', key_segment, value_segment)  15.2 us
  transfers between devices with their start and end apart: 6, of which 4 were waited for; matrix products, arithmetic and copies ran while one was open for 21% of the time, Pallas kernels for 0%

commit v1 on v0

--- a/solution.py
+++ b/solution.py
@@ -13,6 +13,12 @@
 EPS = 1e-06
 GATE_NORM = 16.0
 ROPE_BASE = 10000.0
+
+
+def gather_by_exchange(x, axis, dim):
+    size = lax.axis_size(axis)
+    repeats = [size if d == dim else 1 for d in range(x.ndim)]
+    return lax.all_to_all(jnp.tile(x, repeats), axis, split_axis=dim, concat_axis=dim, tiled=True)
 
 
 def gathered_once(array, axis):
@@ -240,7 +246,7 @@
         fill_slots(normed, routes, experts, capacity), SP, split_axis=0, concat_axis=0, tiled=True
     )
     fanned, shared_flat = (
-        lax.all_gather(arrived.reshape(experts * capacity, model_width), "tp", axis=0, tiled=True),
+        gather_by_exchange(arrived.reshape(experts * capacity, model_width), "tp", 0),
         lax.all_gather(normed, "tp", axis=0, tiled=True),
     )
     routed_rows = fanned.reshape(groups, experts * capacity, model_width)

time: 557 us -> 600 us (1.077)
  waiting for transfers between devices: 197 us -> 223 us
  local copies, waits for them, and re-layouts: 119 us -> 129 us
    all_gather x1 -> x0, waiting for transfers between devices: 55.2 us -> none  [body(): lax.all_gather(arrived.reshape(experts * capacity, model_width), 'tp', ax...]
    all_gather x1, waiting for transfers between devices: 0.02 us -> 48.6 us  [body(): lax.all_gather(normed, 'tp', axis=0, tiled=True)]
    all_to_all x0 -> x1, waiting for transfers between devices: none -> 30 us  [gather_by_exchange(): lax.all_to_all(jnp.tile(x, repeats), axis, split_axis=dim, concat_axis=di...]
    another operation x11 -> x13, local copies, waits for them, and re-layouts: 2.18 us -> 8.48 us  [the longest x2 6.29 us: gather_by_exchange(): jnp.tile(x, repeats)]
  transfers between devices with their start and end apart: 6 -> 6, of which waited for: 4 -> 5; matrix products, arithmetic and copies ran while one was open for 21% -> 14% of each run, Pallas kernels for 0% -> 0%
where the time goes in v1:
time: 600 us; the launch traced here: 596 us
  waiting for transfers between devices  223 us (37%)
  local copies, waits for them, and re-layouts  129 us (22%)
  blocking collectives  102 us (17%)
  matrix products  58.9 us (10%)
  other arithmetic  46.1 us (8%)
  starting transfers between devices  20.8 us (3%)
  between operations  14.2 us (2%)
    reduce_scatter x1, waiting for transfers between devices, body(): lax.psum_scatter(jnp.concatenate([routed_out, shared_out], axis=1).reshap...  85.7 us
    all_to_all x1, blocking collectives, body(): lax.all_to_all(fill_slots(normed, routes, experts, capacity), SP, split_a...  59.6 us
    all_to_all x1, waiting for transfers between devices, body(): lax.all_to_all(routed_done, SP, split_axis=0, concat_axis=0, tiled=True)  51 us
    all_gather x1, waiting for transfers between devices, body(): lax.all_gather(normed, 'tp', axis=0, tiled=True)  48.6 us
    all_gather x3, blocking collectives, gathered_once(): both, at, found = (lax.all_gather(jnp.concatenate(lines), axis), 0, {})  42.5 us
    scatter x2, local copies, waits for them, and re-layouts, fill_slots(): return buffer.at[flat_ids, slot_ids].set(row_data[token_ids])  34.5 us
    all_to_all x1, waiting for transfers between devices, gather_by_exchange(): lax.all_to_all(jnp.tile(x, repeats), axis, split_axis=dim, concat_axis=di...  30 us
    dynamic_slice x32, local copies, waits for them, and re-layouts, blockwise(): lax.scan(advance, start_state, (query_in, key_out, value_blocks, block_de...  20.8 us
  transfers between devices with their start and end apart: 6, of which 5 were waited for; matrix products, arithmetic and copies ran while one was open for 14% of the time, Pallas kernels for 0%

profile of v1, /device:TPU:2, one launch (start us, length us, event | category | flops | bytes accessed | tf_op | source)
XLA Modules:
  0.0 596.0 jit_solution(3797281658250425025)
XLA Ops:
  10.0 13.0 %fusion.178 = f32[8,64,2,64]{3,0,1,2:T(8,128)S(1)} fusion(f32[8,64,2,64]{3,0,1,2:T(8,128)S(1)} %copy.134), kind=kOutput, calls=%fused_computation.308 | output fusion | flops 4128768 | bytes 524288 | tf_op jit(solution)/shard_map/jit(cumsum)/reduce_window_sum | solution.py:122
  36.9 24.3 %while.40 = (s32[]{:T(128)}, f32[2,64,128]{2,1,0:T(8,128)S(1)}, f32[8,64,2,128]{3,1,2,0:T(8,128)}, f32[8,2,64]{2,0,1:T(8,128)S(1)}, f32[8,64,2,64]{3,0,1,2:T(8,1...) while((s32[]{:T(128)}, f32[2,64,128]{2,1,0:T(8,128)S(1)}, ...), condition=%wide.region_2.3_spmd.clone, body=%wide.region_1.2_spmd.clone.sunk | while | flops 4259843 | bytes 494192 | solution.py:143
  63.7 3.1 rev.15
  90.3 24.4 %while.42 = (s32[]{:T(128)}, f32[2,64,128]{2,1,0:T(8,128)S(1)}, f32[8,64,2,128]{3,1,2,0:T(8,128)}, f32[8,2,64]{2,0,1:T(8,128)S(1)}, f32[8,64,2,64]{3,0,1,2:T(8,1...) while((s32[]{:T(128)}, f32[2,64,128]{2,1,0:T(8,128)S(1)}, ...), condition=%wide.region_10.11_spmd.clone, body=%wide.region_9.10_spmd.clone.sunk | while | flops 4259843 | bytes 494192 | solution.py:143
  116.8 12.2 %all-gather.6 = bf16[4,129,128]{2,1,0:T(8,128)(2,1)S(1)} all-gather(bf16[1,129,128]{2,1,0:T(8,128)(2,1)S(1)} %maximum_bitcast_fusion.2), channel_id=4, replica_groups=mesh['sp_0'=8,'sp_1'=4,'sp_2'=2,'tp'=4] {'sp_1'}, dimensions={0}, use_global_device_ids=true | all-gather | bytes 165120 | tf_op jit(solution)/shard_map/all_gather | solution.py:32
  130.8 28.4 %all-gather.7 = bf16[8,129,128]{2,1,0:T(8,128)(2,1)S(1)} all-gather(bf16[1,129,128]{2,1,0:T(8,128)(2,1)S(1)} %maximum_bitcast_fusion.3), channel_id=5, replica_groups=mesh['sp_0'=8,'sp_1'=4,'sp_2'=2,'tp'=4] {'sp_0'}, dimensions={0}, use_global_device_ids=true | all-gather | bytes 297216 | tf_op jit(solution)/shard_map/all_gather | solution.py:32
  182.2 8.8 %while.41 = (s32[]{:T(128)}, f32[2,64,128]{2,1,0:T(8,128)S(1)}, s32[]{:T(128)}, bf16[64,2,64]{2,1,0:T(2,128)(2,1)S(1)}, bf16[64,2,64,128]{3,2,1,0:T(8,128)(2,1)S(1)}, /*index=5*/s32[]{:T(128)}, s32[]{:T(128)}) while((s32[]{:T(128)}, f32[2,64,128]{2,1,0:T(8,128)S(1)}, s32[]{:T(128)}, bf16[64,2,64]{2,1,0:T(2,128)(2,1)S(1)}, ...), condition=%wide.region_5.6_spmd.clone, body=%wide.region_4.5_spmd.clone.sunk | while | flops 82052 | bytes 165225 | solution.py:64
  194.0 4.4 all-to-all-start
  198.4 6.7 %all-to-all-done = bf16[4,128,256]{2,1,0:T(8,128)(2,1)S(1)} async-done(((bf16[4,128,256]{2,1,0:T(8,128)(2,1)}), bf16[4,128,256]{2,1,0:T(8,128)(2,1)S(1)}, u32[]{:S(2)}, u32[]{:S(2)}) %all-to-all-start) | async-done | bytes 262176 | tf_op jit(solution)/shard_map/all_to_all | solution.py:237
  212.3 33.6 %scatter_fusion = bf16[64,6,2048]{2,0,1:T(8,128)(2,1)S(1)} fusion(bf16[64,6,2048]{2,0,1:T(8,128)(2,1)S(1)} %broadcast_in_dim.40, s32[256]{0:T(256)S(1)} %bitcast.316, bf16[256,2048]{1,0:T(8,128)(2,1)} %gather_fusion), kind=kCustom, calls=%fused_computation.2 | custom fusion | bytes 3147776 | tf_op jit(solution)/shard_map/scatter | solution.py:177
  246.8 59.6 %all_to_all.38 = bf16[64,6,2048]{2,1,0:T(8,128)(2,1)S(1)} all-to-all(bf16[64,6,2048]{2,1,0:T(8,128)(2,1)S(1)} %copy.181), channel_id=1, replica_groups=mesh['sp_0'=8,'sp_1'=4,'sp_2'=2,'tp'=4] {'sp_0','sp_1','sp_2'}, dimensions={0} | all-to-all | bytes 3145728 | tf_op jit(solution)/shard_map/all_to_all | solution.py:245
  307.8 4.9 tile.9
  312.7 5.2 all-to-all-start.2
  318.9 48.6 %all-gather.11.cloned.1.call-done = bf16[512,2048]{1,0:T(8,128)(2,1)} async-done(((bf16[128,2048]{1,0:T(8,128)(2,1)}), bf16[512,2048]{1,0:T(8,128)(2,1)}) %all-gather.11.cloned.1.call-update) | async-done | bytes 2097168 | tf_op jit(solution)/shard_map/all_gather | solution.py:250
  370.0 4.8 convolution_convert_fusion.1
  374.9 30.0 %all-to-all-done.2 = bf16[4,384,2048]{2,1,0:T(8,128)(2,1)} async-done(((bf16[4,384,2048]{2,1,0:T(8,128)(2,1)}), bf16[4,384,2048]{2,1,0:T(8,128)(2,1)}, u32[]{:S(2)}, u32[]{:S(2)}) %all-to-all-start.2) | async-done | bytes 6291488 | tf_op jit(solution)/shard_map/all_to_all | solution.py:21
  404.8 5.0 fusion.32
  409.9 4.8 fusion.17
  414.7 4.5 convolution_convert_fusion
  419.2 7.6 %pad_maximum_fusion = bf16[4,512,2048]{2,1,0:T(8,128)(2,1)} fusion(bf16[4,128,2048]{2,1,0:T(8,128)(2,1)S(1)} %bitcast.317, bf16[4,384,2048]{2,1,0:T(8,128)(2,1)} %convolution_convert_fusion), kind=kLoop, calls=%fused_computation.32 | loop fusion | flops 16777216 | bytes 16777216 | tf_op jit(solution)/shard_map/concatenate | solution.py:265
  426.9 85.7 %reduce-scatter.2.cloned.1.call-done = bf16[512,2048]{1,0:T(8,128)(2,1)} async-done(((bf16[2048,2048]{1,0:T(8,128)(2,1)}), bf16[512,2048]{1,0:T(8,128)(2,1)}) %reduce-scatter.2.cloned.1.call-update) | async-done | bytes 2097168 | tf_op jit(solution)/shard_map/reduce_scatter | solution.py:264
  515.6 10.9 %all-to-all-start.3 = ((bf16[64,6,2048]{2,1,0:T(8,128)(2,1)}), bf16[64,6,2048]{2,1,0:T(8,128)(2,1)}, u32[]{:S(2)}, u32[]{:S(2)}) async-start(bf16[64,6,2048]{2,1,0:T(8,128)(2,1)} %reshape.773), calls=%async_computation.4 | async-start | bytes 4194304 | tf_op jit(solution)/shard_map/all_to_all | solution.py:275
  526.5 51.0 %all-to-all-done.3 = bf16[64,6,2048]{2,1,0:T(8,128)(2,1)} async-done(((bf16[64,6,2048]{2,1,0:T(8,128)(2,1)}), bf16[64,6,2048]{2,1,0:T(8,128)(2,1)}, u32[]{:S(2)}, u32[]{:S(2)}) %all-to-all-start.3) | async-done | bytes 1572896 | tf_op jit(solution)/shard_map/all_to_all | solution.py:275
  584.9 3.2 multiply_reduce_fusion
  (433 shorter events, 151.9 us)
Async XLA Ops:
  6.5 408.2 %copy-start = (bf16[1,256,2048]{2,1,0:T(8,128)(2,1)S(1)}, bf16[1,256,2048]{2,1,0:T(8,128)(2,1)}, u32[]{:S(2)}) copy-start(bf16[1,256,2048]{2,1,0:T(8,128)(2,1)} %param.42) | copy-start | bytes 3145732
  6.5 173.0 %all-gather.13.cloned.1.call-start = ((), (), s32[]{:S(2)}) async-start(), calls=%async_computation.7 | async-start | bytes 2263040 | tf_op jit(solution)/shard_map/all_gather | solution.py:32
  9.2 13.9 %copy-start.23 = (bf16[512,128]{1,0:T(8,128)(2,1)S(1)}, bf16[512,128]{1,0:T(8,128)(2,1)}, u32[]{:S(2)}) copy-start(bf16[512,128]{1,0:T(8,128)(2,1)} %param.27) | copy-start | bytes 393220
  9.2 14.1 %copy-start.24 = (bf16[512,128]{1,0:T(8,128)(2,1)S(1)}, bf16[512,128]{1,0:T(8,128)(2,1)}, u32[]{:S(2)}) copy-start(bf16[512,128]{1,0:T(8,128)(2,1)} %param.28) | copy-start | bytes 393220
  9.6 13.5 %copy-start.7 = (f32[512,128]{0,1:T(8,128)}, f32[512,128]{0,1:T(8,128)S(1)}, u32[]{:S(2)}) copy-start(f32[512,128]{0,1:T(8,128)S(1)} %get-tuple-element.357) | copy-start | bytes 786436
  9.6 60.3 %copy-start.9 = (f32[512,128]{0,1:T(8,128)}, f32[512,128]{0,1:T(8,128)S(1)}, u32[]{:S(2)}) copy-start(f32[512,128]{0,1:T(8,128)S(1)} %get-tuple-element.416) | copy-start | bytes 786436
  23.9 5.2 copy-start.15
  23.9 5.2 copy-start.16
  63.7 11.0 %copy-start.33 = (s32[128,2]{0,1:T(2,128)S(1)}, s32[128,2]{0,1:T(2,128)}, u32[]{:S(2)}) copy-start(s32[128,2]{0,1:T(2,128)} %param.38) | copy-start | bytes 3076
  90.3 74.8 %copy-start.25 = (f32[8,2,64]{2,0,1:T(8,128)S(1)}, f32[8,2,64]{2,0,1:T(8,128)}, u32[]{:S(2)}) copy-start(f32[8,2,64]{2,0,1:T(8,128)} %get-tuple-element.374) | copy-start | bytes 12292
  129.0 36.1 %copy-start.17 = (bf16[4,129,128]{2,1,0:T(8,128)(2,1)}, bf16[4,129,128]{2,1,0:T(8,128)(2,1)S(1)}, u32[]{:S(2)}) copy-start(bf16[4,129,128]{2,1,0:T(8,128)(2,1)S(1)} %all-gather.6) | copy-start | bytes 396292
  129.9 40.9 %copy-start.31 = (f32[2,64]{1,0:T(2,128)}, f32[2,64]{1,0:T(2,128)S(1)}, u32[]{:S(2)}) copy-start(f32[2,64]{1,0:T(2,128)S(1)} %reshape.807) | copy-start | bytes 1540
  130.6 40.2 %copy-start.32 = (f32[2,64]{1,0:T(2,128)}, f32[2,64]{1,0:T(2,128)S(1)}, u32[]{:S(2)}) copy-start(f32[2,64]{1,0:T(2,128)S(1)} %reshape.809) | copy-start | bytes 1540
  170.9 4.8 copy-start.8
  171.0 7.4 %copy-start.29 = (s32[2,128]{1,0:T(2,128)S(1)}, s32[2,128]{1,0:T(2,128)}, u32[]{:S(2)}) copy-start(s32[2,128]{1,0:T(2,128)} %eq.36) | copy-start | bytes 3076
  180.6 12.2 %copy-start.34 = (f32[256]{0:T(256)S(1)}, f32[256]{0:T(256)}, u32[]{:S(2)}) copy-start(f32[256]{0:T(256)} %param.33) | copy-start | bytes 3076
  192.8 5.6 copy-start.30
  194.0 11.1 %all-to-all-start = ((bf16[4,128,256]{2,1,0:T(8,128)(2,1)}), bf16[4,128,256]{2,1,0:T(8,128)(2,1)S(1)}, u32[]{:S(2)}, u32[]{:S(2)}) async-start(bf16[4,128,256]{2,1,0:T(8,128)(2,1)} %bitcast.62), calls=%async_computation | async-start | bytes 524288 | tf_op jit(solution)/shard_map/all_to_all | solution.py:237
  312.7 92.2 %all-to-all-start.2 = ((bf16[4,384,2048]{2,1,0:T(8,128)(2,1)}), bf16[4,384,2048]{2,1,0:T(8,128)(2,1)}, u32[]{:S(2)}, u32[]{:S(2)}) async-start(bf16[4,384,2048]{2,1,0:T(8,128)(2,1)} %tile.9), calls=%async_computation.2 | async-start | bytes 12582912 | tf_op jit(solution)/shard_map/all_to_all | solution.py:21
  317.9 49.6 %all-gather.11.cloned.1.call-start = ((), (), s32[]{:S(2)}) async-start(), calls=%async_computation.5 | async-start | bytes 2621440 | tf_op jit(solution)/shard_map/all_gather | solution.py:250
  318.6 193.9 %reduce-scatter.2.cloned.1.call-start = ((), (), s32[]{:S(2)}) async-start(), calls=%async_computation.6 | async-start | bytes 10485760 | tf_op jit(solution)/shard_map/reduce_scatter | solution.py:264
  404.8 5.0 copy-start.42
  515.6 10.9 %copy-start.35 = (f32[128,2]{0,1:T(2,128)S(1)}, f32[128,2]{0,1:T(2,128)}, u32[]{:S(2)}) copy-start(f32[128,2]{0,1:T(2,128)} %param.39) | copy-start | bytes 3076
  515.6 62.0 %all-to-all-start.3 = ((bf16[64,6,2048]{2,1,0:T(8,128)(2,1)}), bf16[64,6,2048]{2,1,0:T(8,128)(2,1)}, u32[]{:S(2)}, u32[]{:S(2)}) async-start(bf16[64,6,2048]{2,1,0:T(8,128)(2,1)} %reshape.773), calls=%async_computation.4 | async-start | bytes 4194304 | tf_op jit(solution)/shard_map/all_to_all | solution.py:275
  (27 other events, 71.0 us)
Sparse Core Ops, SparseCore 0:
  62.0 79.5 all-gather.12
  320.5 46.9 all-gather.10
  427.0 85.5 reduce-scatter.1
